TPU v7x, 32 devices: a whole 2x2x4 slice. The times are simulated.
32 devices in a mesh: kv: 8 (over z, y), tp: 4 (over x, core).
Axes of the slice: x: 2, y: 2, z: 4, core: 2. Of those that a mesh axis runs over, the one named last changes fastest.
Arguments:
- tokens: bfloat16 [4096, 2048], P('kv'), may hold values from -18 to 18
- w_query: bfloat16 [2048, 1024], P(None, 'tp'), may hold values from -0.125 to 0.125
- w_key: bfloat16 [2048, 256], P(None, 'tp'), may hold values from -0.125 to 0.125
- w_value: bfloat16 [2048, 256], P(None, 'tp'), may hold values from -18 to 18
- w_out: bfloat16 [1024, 2048], P(None, 'tp'), may hold values from -0.1875 to 0.1875
- out_gain: float32 [1024], replicated, may hold values from 0.1 to 1.9
- chosen: int32 [4, 64, 8], P('tp', 'kv'), may hold values from -1 to 63, as said below
Outputs:
- mixed_out: bfloat16 [4096, 2048], P('kv', 'tp')
Inputs may be any that keep to these rules, and one draw needn't show every extreme that they name: chosen[h, b, 0] is b itself; the other entries of a row are distinct key blocks lying wholly before block b, or -1, placed after all named blocks; for each key head h, the query blocks on one index of kv (its 512 positions) name, together, at most one key block of head h held by any other index of kv.
All inputs are finite; a program needn't handle non-finite values.
Results may differ from a plain program's by a relative error of at most 0.024.
Values may be sent and summed in bfloat16 or wider, within the bound.
No kernel may reach another device: no remote copies, remote signals or barrier semaphores. Data moves between devices by JAX's collectives and lax.ppermute only.
A program may use at most 64 MiB of HBM per device.

v0:
```python
import jax
import jax.numpy as jnp
from jax import lax
from jax.sharding import PartitionSpec as P

HQ = 16
HD = 64
BLK = 64
SEL = 8
rope_base = 500000.0
norm_eps = 1e-06


def rotate(vectors, positions):
    half_size = vectors.shape[-1] // 2
    frequency = rope_base ** (-jnp.arange(half_size, dtype=jnp.float32) / half_size)
    angles = positions.astype(jnp.float32)[:, None] * frequency[None, :]
    cosine = jnp.cos(angles)[:, None, :]
    sine_wave = jnp.sin(angles)[:, None, :]
    lower_half = vectors[..., :half_size]
    upper_half = vectors[..., half_size:]
    return jnp.concatenate(
        [
            lower_half * cosine - upper_half * sine_wave,
            upper_half * cosine + lower_half * sine_wave,
        ],
        axis=-1,
    )


def per_device(tokens, w_query, w_key, w_value, w_out, out_gain, chosen):
    count_kv = lax.axis_size("kv")
    kv_place = lax.axis_index("kv")
    row_count = tokens.shape[0]
    block_count = row_count // BLK
    feat_width = w_query.shape[1]
    head_count = feat_width // HD
    positions = kv_place * row_count + jnp.arange(row_count, dtype=jnp.int32)
    queries = rotate(
        jnp.dot(tokens, w_query, preferred_element_type=jnp.float32).reshape(
            row_count, head_count, HD
        ),
        positions,
    ).astype(jnp.bfloat16)
    key_rows = (
        rotate(
            jnp.dot(tokens, w_key, preferred_element_type=jnp.float32).reshape(row_count, 1, HD),
            positions,
        )
        .astype(jnp.bfloat16)
        .reshape(row_count, HD)
    )
    value_rows = jnp.dot(tokens, w_value, preferred_element_type=jnp.float32).astype(jnp.bfloat16)
    local_pairs = jnp.concatenate([key_rows, value_rows], axis=1).reshape(block_count, BLK, 2 * HD)
    chosen_ids = chosen[0]
    usable = chosen_ids >= 0
    owners = jnp.where(usable, chosen_ids // block_count, kv_place)
    local_index = jnp.where(usable, chosen_ids % block_count, 0)
    remote = usable & (owners != kv_place)
    peer_ids = jnp.arange(count_kv, dtype=jnp.int32)
    matches = remote[:, :, None] & (owners[:, :, None] == peer_ids[None, None, :])
    wanted = jnp.max(jnp.where(matches, local_index[:, :, None], -1), axis=(0, 1))
    asked_for = lax.all_to_all(
        wanted.reshape(count_kv, 1), "kv", split_axis=0, concat_axis=0, tiled=True
    )[:, 0]
    outgoing = jnp.where(
        (asked_for >= 0)[:, None, None],
        local_pairs[jnp.maximum(asked_for, 0)],
        jnp.zeros((), jnp.bfloat16),
    )
    arrived = lax.all_to_all(outgoing, "kv", split_axis=0, concat_axis=0, tiled=True)
    pool_pairs = jnp.concatenate([arrived, local_pairs], axis=0)
    slot_index = jnp.where(owners == kv_place, count_kv + local_index, owners)
    selected = pool_pairs[slot_index]
    pair_count = block_count // 2
    offsets = jnp.arange(BLK, dtype=jnp.int32)
    score_scale = HD ** (-0.5)

    def attend(bundle):
        query_part, stacked, pair_ids, pair_usable, query_pos = bundle
        key_part = stacked[..., :HD]
        value_part = stacked[..., HD:]
        scores = (
            jnp.einsum("pqhd,pskd->phqsk", query_part, key_part, preferred_element_type=jnp.float32)
            * score_scale
        )
        key_pos = pair_ids[:, :, None] * BLK + offsets
        allowed = pair_usable[:, None, :, None] & (
            key_pos[:, None, :, :] <= query_pos[:, :, None, None]
        )
        scores = jnp.where(allowed[:, None], scores, -jnp.inf)
        peak_score = jnp.max(scores, axis=(3, 4), keepdims=True)
        weights = jnp.exp(scores - peak_score)
        softmax_w = (weights / jnp.sum(weights, axis=(3, 4), keepdims=True)).astype(jnp.bfloat16)
        mixed_out = jnp.einsum(
            "phqsk,pskd->pqhd", softmax_w, value_part, preferred_element_type=jnp.float32
        )
        return mixed_out.astype(jnp.bfloat16)

    attended = lax.map(
        attend,
        (
            queries.reshape(pair_count, 2, BLK, head_count, HD),
            selected.reshape(pair_count, 2, SEL, BLK, 2 * HD),
            chosen_ids.reshape(pair_count, 2, SEL),
            usable.reshape(pair_count, 2, SEL),
            positions.reshape(pair_count, 2, BLK),
        ),
    ).reshape(row_count, feat_width)
    attn_f32 = attended.astype(jnp.float32)
    squares = lax.psum(jnp.sum(attn_f32 * attn_f32, axis=1), "tp")
    gain_part = lax.dynamic_slice_in_dim(out_gain, lax.axis_index("tp") * feat_width, feat_width)
    scaled = (attn_f32 * gain_part[None, :]).astype(jnp.bfloat16)
    product = jnp.dot(
        lax.all_gather(scaled, "tp", axis=1, tiled=True), w_out, preferred_element_type=jnp.float32
    )
    inverse = lax.rsqrt(squares / (HQ * HD) + norm_eps)
    return (inverse[:, None] * product).astype(jnp.bfloat16)


def solution(mesh):
    return jax.shard_map(
        per_device,
        mesh=mesh,
        in_specs=(
            P("kv", None),
            P(None, "tp"),
            P(None, "tp"),
            P(None, "tp"),
            P(None, "tp"),
            P(),
            P("tp", "kv", None),
        ),
        out_specs=P("kv", "tp"),
        check_vma=False,
    )
```

profile of v0, /device:TPU:0, one launch (start us, length us, event | category | flops | bytes accessed | tf_op | source)
XLA Modules:
  0.0 87.1 jit_solution(12271367534152278380)
XLA Ops:
  6.5 0.8 fusion.20
  7.4 0.7 compare_and_fusion.1
  8.2 0.7 copy.36
  8.9 7.3 %all-to-all-start = ((s32[8,1,1]{2,1,0:T(1,128)}), s32[8,1,1]{2,1,0:T(1,128)S(1)}, u32[]{:S(2)}, u32[]{:S(2)}) async-start(s32[8,1,1]{2,1,0:T(1,128)} %copy.36), calls=%async_computation | async-start | bytes 8192 | tf_op jit(solution)/shard_map/all_to_all | solution.py:63
  16.2 0.7 compare_select_fusion
  16.9 1.7 %convolution_bitcast_fusion.1 = f32[512,1,64]{0,2,1:T(8,128)S(1)} fusion(bf16[512,2048]{1,0:T(8,128)(2,1)S(1)} %copy-done, bf16[2048,64]{0,1:T(8,128)(2,1)} %param.11), kind=kOutput, calls=%fused_computation.26 | convolution fusion | flops 134217728 | bytes 2490368 | tf_op jit(solution)/shard_map/dot_general | solution.py:47
  19.6 0.8 convolution_convert_fusion
  20.4 2.0 %fusion.34 = f32[512,256]{0,1:T(8,128)S(1)} fusion(bf16[512,2048]{1,0:T(8,128)(2,1)S(1)} %copy-done, bf16[2048,256]{1,0:T(8,128)(2,1)} %param.10), kind=kOutput, calls=%fused_computation.93 | convolution fusion | flops 536870912 | bytes 3670016 | tf_op jit(solution)/shard_map/dot_general | solution.py:40
  22.9 1.6 %pad_maximum_fusion = bf16[4,2,64,4,64]{2,1,0,4,3:T(2,128)(2,1)} fusion(bf16[4,2,64,4,32]{2,1,0,4,3:T(2,128)(2,1)S(1)} %concatenate.35, bf16[4,2,64,4,32]{2,1,0,4,3:T(2,128)(2,1)S(1)} %concatenate.34), kind=kLoop, calls=%fused_computation.29 | loop fusion | flops 131072 | bytes 524288 | tf_op jit(solution)/shard_map/concatenate | solution.py:22
  25.9 0.7 broadcast_select_fusion
  26.6 6.0 %all-to-all-start.1 = ((bf16[8,64,128]{2,1,0:T(8,128)(2,1)}), bf16[8,64,128]{2,1,0:T(8,128)(2,1)S(1)}, u32[]{:S(2)}, u32[]{:S(2)}) async-start(bf16[8,64,128]{2,1,0:T(8,128)(2,1)} %broadcast_select_fusion), calls=%async_computation.1 | async-start | bytes 262144 | tf_op jit(solution)/shard_map/all_to_all | solution.py:71
  32.7 0.8 dynamic_slice.23
  33.4 6.5 %all-to-all-done.1 = bf16[8,64,128]{2,1,0:T(8,128)(2,1)S(1)} async-done(((bf16[8,64,128]{2,1,0:T(8,128)(2,1)}), bf16[8,64,128]{2,1,0:T(8,128)(2,1)S(1)}, u32[]{:S(2)}, u32[]{:S(2)}) %all-to-all-start.1) | async-done | bytes 131104 | tf_op jit(solution)/shard_map/all_to_all | solution.py:71
  40.1 0.7 gather_fusion.1
  40.8 17.1 %while.11 = (s32[]{:T(128)}, bf16[4,2,64,4,64]{2,4,3,1,0:T(8,128)(2,1)}, bf16[4,2,8,64,128]{4,3,2,1,0:T(8,128)(2,1)S(1)}, pred[4,2,8]{2,1,0:T(4,128)(4,1)S(1)}, ...) while((s32[]{:T(128)}, ...), condition=%wide.region_4.5_spmd.clone, body=%wide.region_1.4_spmd.clone.sunk | while | flops 69369872 | bytes 13193617 | solution.py:100
  41.8 1.0 %constant_dynamic-slice_fusion.4 = bf16[1,2,64,4,64]{2,1,0,4,3:T(2,128)(2,1)S(1)} fusion(bf16[4,2,64,4,64]{2,1,0,4,3:T(2,128)(2,1)} %get-tuple-element.185, s32[]{:T(128)} %get-tuple-element.171), kind=kLoop, calls=%fused_computation.18.clone.1 | loop fusion | bytes 131076 | tf_op jit(solution)/shard_map/while/body/jit(dynamic_index_in_dim)/dynamic_slice | solution.py:100
  43.9 1.2 %fusion.52 = bf16[4,2,64,4,64]{2,4,3,1,0:T(8,128)(2,1)} fusion(bf16[4,2,64,4,64]{2,4,3,1,0:T(8,128)(2,1)} %get-tuple-element.172, s32[]{:T(128)} %get-tuple-element.171, f32[2,4,64,8,64]{2,4,1,3,0:T(8,128)S(1)} %get-tuple-element.161, f32[2,4,64]{2,1,0:T(4,128)S(1)} %fusion.51, f32[2,4,64]{2,1,0:T(4,128)S(1)} %get-tuple-element.162, ...), kind=kOutput, calls=%fused_computation.10.clone.1 | convolution fusion | flops 34373632 | bytes 1446400 | tf_op jit(solution)/shard_map/while/body/eval_jaxpr/phqsk,pskd->pqhd/dot_general | solution.py:95
  46.1 1.0 %constant_dynamic-slice_fusion.4 = bf16[1,2,64,4,64]{2,1,0,4,3:T(2,128)(2,1)S(1)} fusion(bf16[4,2,64,4,64]{2,1,0,4,3:T(2,128)(2,1)} %get-tuple-element.185, s32[]{:T(128)} %get-tuple-element.171), kind=kLoop, calls=%fused_computation.18.clone.1 | loop fusion | bytes 131076 | tf_op jit(solution)/shard_map/while/body/jit(dynamic_index_in_dim)/dynamic_slice | solution.py:100
  48.1 1.2 %fusion.52 = bf16[4,2,64,4,64]{2,4,3,1,0:T(8,128)(2,1)} fusion(bf16[4,2,64,4,64]{2,4,3,1,0:T(8,128)(2,1)} %get-tuple-element.172, s32[]{:T(128)} %get-tuple-element.171, f32[2,4,64,8,64]{2,4,1,3,0:T(8,128)S(1)} %get-tuple-element.161, f32[2,4,64]{2,1,0:T(4,128)S(1)} %fusion.51, f32[2,4,64]{2,1,0:T(4,128)S(1)} %get-tuple-element.162, ...), kind=kOutput, calls=%fused_computation.10.clone.1 | convolution fusion | flops 34373632 | bytes 1446400 | tf_op jit(solution)/shard_map/while/body/eval_jaxpr/phqsk,pskd->pqhd/dot_general | solution.py:95
  49.7 0.6 copy-done.1
  50.4 1.0 %constant_dynamic-slice_fusion.4 = bf16[1,2,64,4,64]{2,1,0,4,3:T(2,128)(2,1)S(1)} fusion(bf16[4,2,64,4,64]{2,1,0,4,3:T(2,128)(2,1)} %get-tuple-element.185, s32[]{:T(128)} %get-tuple-element.171), kind=kLoop, calls=%fused_computation.18.clone.1 | loop fusion | bytes 131076 | tf_op jit(solution)/shard_map/while/body/jit(dynamic_index_in_dim)/dynamic_slice | solution.py:100
  52.4 1.2 %fusion.52 = bf16[4,2,64,4,64]{2,4,3,1,0:T(8,128)(2,1)} fusion(bf16[4,2,64,4,64]{2,4,3,1,0:T(8,128)(2,1)} %get-tuple-element.172, s32[]{:T(128)} %get-tuple-element.171, f32[2,4,64,8,64]{2,4,1,3,0:T(8,128)S(1)} %get-tuple-element.161, f32[2,4,64]{2,1,0:T(4,128)S(1)} %fusion.51, f32[2,4,64]{2,1,0:T(4,128)S(1)} %get-tuple-element.162, ...), kind=kOutput, calls=%fused_computation.10.clone.1 | convolution fusion | flops 34373632 | bytes 1446400 | tf_op jit(solution)/shard_map/while/body/eval_jaxpr/phqsk,pskd->pqhd/dot_general | solution.py:95
  54.0 0.6 copy-done.1
  54.7 1.0 %constant_dynamic-slice_fusion.4 = bf16[1,2,64,4,64]{2,1,0,4,3:T(2,128)(2,1)S(1)} fusion(bf16[4,2,64,4,64]{2,1,0,4,3:T(2,128)(2,1)} %get-tuple-element.185, s32[]{:T(128)} %get-tuple-element.171), kind=kLoop, calls=%fused_computation.18.clone.1 | loop fusion | bytes 131076 | tf_op jit(solution)/shard_map/while/body/jit(dynamic_index_in_dim)/dynamic_slice | solution.py:100
  56.7 1.2 %fusion.52 = bf16[4,2,64,4,64]{2,4,3,1,0:T(8,128)(2,1)} fusion(bf16[4,2,64,4,64]{2,4,3,1,0:T(8,128)(2,1)} %get-tuple-element.172, s32[]{:T(128)} %get-tuple-element.171, f32[2,4,64,8,64]{2,4,1,3,0:T(8,128)S(1)} %get-tuple-element.161, f32[2,4,64]{2,1,0:T(4,128)S(1)} %fusion.51, f32[2,4,64]{2,1,0:T(4,128)S(1)} %get-tuple-element.162, ...), kind=kOutput, calls=%fused_computation.10.clone.1 | convolution fusion | flops 34373632 | bytes 1446400 | tf_op jit(solution)/shard_map/while/body/eval_jaxpr/phqsk,pskd->pqhd/dot_general | solution.py:95
  57.9 1.3 %copy.41 = f32[4,2,64,4,64]{4,3,2,1,0:T(4,128)S(1)} copy(bf16[4,2,64,4,64]{2,4,3,1,0:T(8,128)(2,1)} %get-tuple-element.47) | data formatting | bytes 786432 | tf_op jit(solution)/shard_map/convert_element_type | solution.py:110
  59.3 1.4 %reshape.350 = f32[512,256]{1,0:T(8,128)} reshape(f32[4,2,64,4,64]{4,3,2,1,0:T(4,128)S(1)} %copy.41) | data formatting | bytes 1048576 | tf_op jit(solution)/shard_map/convert_element_type | solution.py:110
  60.7 1.8 %multiply_convert_fusion = bf16[512,256]{1,0:T(8,128)(2,1)} fusion(f32[512,256]{1,0:T(8,128)} %reshape.350, f32[256]{0:T(256)S(1)} %dynamic_slice.23), kind=kLoop, calls=%fused_computation.30 | loop fusion | flops 262144 | bytes 787456 | tf_op jit(solution)/shard_map/convert_element_type | solution.py:113
  62.5 1.2 %multiply_reduce_fusion = f32[4,2,64]{2,1,0:T(2,128)S(1)} fusion(bf16[4,2,64,4,64]{2,4,3,1,0:T(8,128)(2,1)} %get-tuple-element.47), kind=kLoop, calls=%fused_computation.28 | loop fusion | flops 392704 | bytes 264192 | tf_op jit(solution)/shard_map/reduce_sum | solution.py:111
  63.8 5.6 %psum.7 = f32[512]{0:T(512)S(1)} all-reduce(f32[512]{0:T(512)S(1)} %reduce_sum.21), channel_id=1, replica_groups=mesh['kv'=8,'tp'=4] {'tp'}, use_global_device_ids=true, to_apply=%region_6.7 | all-reduce | flops 512 | bytes 4096 | tf_op jit(solution)/shard_map/psum | solution.py:111
  69.4 7.8 %all-gather.2.cloned.1.call-done = bf16[512,1024]{1,0:T(8,128)(2,1)} async-done(((bf16[512,256]{1,0:T(8,128)(2,1)}), bf16[512,1024]{1,0:T(8,128)(2,1)}) %all-gather.2.cloned.1.call-update) | async-done | bytes 1048592 | tf_op jit(solution)/shard_map/all_gather | solution.py:115
  77.3 3.0 %fusion.10 = bf16[512,512]{1,0:T(8,128)(2,1)} fusion(bf16[512,1024]{1,0:T(8,128)(2,1)} %all-gather.2.cloned.1.call-done, bf16[1024,512]{1,0:T(8,128)(2,1)} %param.13, f32[512]{0:T(512)S(1)} %add_rsqrt_fusion), kind=kOutput, calls=%fused_computation.25 | convolution fusion | flops 537395200 | bytes 2623488 | tf_op jit(solution)/shard_map/dot_general | solution.py:114
  (83 shorter events, 9.9 us)
Async XLA Ops:
  6.5 10.4 %copy-start = (bf16[512,2048]{1,0:T(8,128)(2,1)S(1)}, bf16[512,2048]{1,0:T(8,128)(2,1)}, u32[]{:S(2)}) copy-start(bf16[512,2048]{1,0:T(8,128)(2,1)} %param.9) | copy-start | bytes 6291460
  6.5 13.0 %copy-start.3 = (bf16[2048,64]{0,1:T(8,128)(2,1)S(1)}, bf16[2048,64]{0,1:T(8,128)(2,1)}, u32[]{:S(2)}) copy-start(bf16[2048,64]{0,1:T(8,128)(2,1)} %param.12) | copy-start | bytes 786436
  8.9 15.9 %all-to-all-start = ((s32[8,1,1]{2,1,0:T(1,128)}), s32[8,1,1]{2,1,0:T(1,128)S(1)}, u32[]{:S(2)}, u32[]{:S(2)}) async-start(s32[8,1,1]{2,1,0:T(1,128)} %copy.36), calls=%async_computation | async-start | bytes 8192 | tf_op jit(solution)/shard_map/all_to_all | solution.py:63
  22.4 11.0 %copy-start.4 = (s32[1,8,8]{2,1,0:T(8,128)S(1)}, s32[1,8,8]{2,1,0:T(8,128)}, u32[]{:S(2)}) copy-start(s32[1,8,8]{2,1,0:T(8,128)} %param.15) | copy-start | bytes 772
  26.6 13.3 %all-to-all-start.1 = ((bf16[8,64,128]{2,1,0:T(8,128)(2,1)}), bf16[8,64,128]{2,1,0:T(8,128)(2,1)S(1)}, u32[]{:S(2)}, u32[]{:S(2)}) async-start(bf16[8,64,128]{2,1,0:T(8,128)(2,1)} %broadcast_select_fusion), calls=%async_computation.1 | async-start | bytes 262144 | tf_op jit(solution)/shard_map/all_to_all | solution.py:71
  32.6 44.7 %all-gather.2.cloned.1.call-start = ((), (), s32[]{:S(2)}) async-start(), calls=%async_computation.2 | async-start | bytes 1310720 | tf_op jit(solution)/shard_map/all_gather | solution.py:115
  40.8 1.0 %copy-start.1 = (bf16[4,2,8,64,128]{4,3,2,1,0:T(8,128)(2,1)}, bf16[4,2,8,64,128]{4,3,2,1,0:T(8,128)(2,1)S(1)}, u32[]{:S(2)}) copy-start(bf16[4,2,8,64,128]{4,3,2,1,0:T(8,128)(2,1)S(1)} %get-tuple-element.181) | copy-start | bytes 3145732 | tf_op jit(solution)/shard_map/while
  43.9 1.2 %copy-start.2 = (bf16[4,2,8,64,128]{4,3,2,1,0:T(8,128)(2,1)S(1)}, bf16[4,2,8,64,128]{4,3,2,1,0:T(8,128)(2,1)}, u32[]{:S(2)}) copy-start(bf16[4,2,8,64,128]{4,3,2,1,0:T(8,128)(2,1)} %copy-done.1) | copy-start | bytes 3145732 | tf_op jit(solution)/shard_map/while
  45.1 1.0 %copy-start.1 = (bf16[4,2,8,64,128]{4,3,2,1,0:T(8,128)(2,1)}, bf16[4,2,8,64,128]{4,3,2,1,0:T(8,128)(2,1)S(1)}, u32[]{:S(2)}) copy-start(bf16[4,2,8,64,128]{4,3,2,1,0:T(8,128)(2,1)S(1)} %get-tuple-element.181) | copy-start | bytes 3145732 | tf_op jit(solution)/shard_map/while
  48.1 1.2 %copy-start.2 = (bf16[4,2,8,64,128]{4,3,2,1,0:T(8,128)(2,1)S(1)}, bf16[4,2,8,64,128]{4,3,2,1,0:T(8,128)(2,1)}, u32[]{:S(2)}) copy-start(bf16[4,2,8,64,128]{4,3,2,1,0:T(8,128)(2,1)} %copy-done.1) | copy-start | bytes 3145732 | tf_op jit(solution)/shard_map/while
  49.4 1.0 %copy-start.1 = (bf16[4,2,8,64,128]{4,3,2,1,0:T(8,128)(2,1)}, bf16[4,2,8,64,128]{4,3,2,1,0:T(8,128)(2,1)S(1)}, u32[]{:S(2)}) copy-start(bf16[4,2,8,64,128]{4,3,2,1,0:T(8,128)(2,1)S(1)} %get-tuple-element.181) | copy-start | bytes 3145732 | tf_op jit(solution)/shard_map/while
  52.4 1.2 %copy-start.2 = (bf16[4,2,8,64,128]{4,3,2,1,0:T(8,128)(2,1)S(1)}, bf16[4,2,8,64,128]{4,3,2,1,0:T(8,128)(2,1)}, u32[]{:S(2)}) copy-start(bf16[4,2,8,64,128]{4,3,2,1,0:T(8,128)(2,1)} %copy-done.1) | copy-start | bytes 3145732 | tf_op jit(solution)/shard_map/while
  53.7 1.0 %copy-start.1 = (bf16[4,2,8,64,128]{4,3,2,1,0:T(8,128)(2,1)}, bf16[4,2,8,64,128]{4,3,2,1,0:T(8,128)(2,1)S(1)}, u32[]{:S(2)}) copy-start(bf16[4,2,8,64,128]{4,3,2,1,0:T(8,128)(2,1)S(1)} %get-tuple-element.181) | copy-start | bytes 3145732 | tf_op jit(solution)/shard_map/while
  56.7 1.2 %copy-start.2 = (bf16[4,2,8,64,128]{4,3,2,1,0:T(8,128)(2,1)S(1)}, bf16[4,2,8,64,128]{4,3,2,1,0:T(8,128)(2,1)}, u32[]{:S(2)}) copy-start(bf16[4,2,8,64,128]{4,3,2,1,0:T(8,128)(2,1)} %copy-done.1) | copy-start | bytes 3145732 | tf_op jit(solution)/shard_map/while
Sparse Core Ops, SparseCore 0:
  62.6 14.5 all-gather.1
where the time goes:
time: 87.9 us; the launch traced here: 87.1 us
  matrix products  14.5 us (16%)
  waiting for transfers between devices  14.3 us (16%)
  local copies, waits for them, and re-layouts  13.6 us (15%)
  between operations  13.6 us (15%)
  starting transfers between devices  13.3 us (15%)
  other arithmetic  11.9 us (14%)
  blocking collectives  5.63 us (6%)
    all_gather x1, waiting for transfers between devices, per_device(): lax.all_gather(scaled, 'tp', axis=1, tiled=True)  7.83 us
    all_to_all x1, starting transfers between devices, per_device(): lax.all_to_all(wanted.reshape(count_kv, 1), 'kv', split_axis=0, concat_ax...  7.31 us
    all_to_all x1, waiting for transfers between devices, per_device(): lax.all_to_all(outgoing, 'kv', split_axis=0, concat_axis=0, tiled=True)  6.5 us
    all_to_all x1, starting transfers between devices, per_device(): lax.all_to_all(outgoing, 'kv', split_axis=0, concat_axis=0, tiled=True)  6 us
    psum x1, blocking collectives, per_device(): squares = lax.psum(jnp.sum(attn_f32 * attn_f32, axis=1), 'tp')  5.63 us
    dot_general x4, matrix products, attend(): jnp.einsum('phqsk,pskd->pqhd', softmax_w, value_part, preferred_element_t...  4.94 us
    dynamic_slice x8, local copies, waits for them, and re-layouts, per_device(): lax.map(attend, (queries.reshape(pair_count, 2, BLK, head_count, HD), sel...  4.53 us
    dot_general x1, matrix products, per_device(): jnp.dot(lax.all_gather(scaled, 'tp', axis=1, tiled=True), w_out, preferre...  3.04 us
  transfers between devices with their start and end apart: 3, of which 2 were waited for; matrix products, arithmetic and copies ran while one was open for 12% of the time, Pallas kernels for 0%

commit v1 on v0

--- a/solution.py
+++ b/solution.py
@@ -112,7 +112,9 @@
     gain_part = lax.dynamic_slice_in_dim(out_gain, lax.axis_index("tp") * feat_width, feat_width)
     scaled = (attn_f32 * gain_part[None, :]).astype(jnp.bfloat16)
     product = jnp.dot(
-        lax.all_gather(scaled, "tp", axis=1, tiled=True), w_out, preferred_element_type=jnp.float32
+        jnp.concatenate(lax.all_gather(scaled, "tp"), axis=1),
+        w_out,
+        preferred_element_type=jnp.float32,
     )
     inverse = lax.rsqrt(squares / (HQ * HD) + norm_eps)
     return (inverse[:, None] * product).astype(jnp.bfloat16)

time: 87.9 us -> 89 us (1.013)
  local copies, waits for them, and re-layouts: 13.6 us -> 15.1 us
    all_gather x0 -> x1, local copies, waits for them, and re-layouts: none -> 1.49 us  [per_device(): lax.all_gather(scaled, 'tp')]
where the time goes in v1:
time: 89 us; the launch traced here: 88.2 us
  local copies, waits for them, and re-layouts  15.1 us (17%)
  matrix products  14.3 us (16%)
  waiting for transfers between devices  14.2 us (16%)
  between operations  13.6 us (15%)
  starting transfers between devices  13.3 us (15%)
  other arithmetic  11.9 us (13%)
  blocking collectives  5.63 us (6%)
    all_gather x1, waiting for transfers between devices, per_device(): lax.all_gather(scaled, 'tp')  7.71 us
    all_to_all x1, starting transfers between devices, per_device(): lax.all_to_all(wanted.reshape(count_kv, 1), 'kv', split_axis=0, concat_ax...  7.31 us
    all_to_all x1, waiting for transfers between devices, per_device(): lax.all_to_all(outgoing, 'kv', split_axis=0, concat_axis=0, tiled=True)  6.5 us
    all_to_all x1, starting transfers between devices, per_device(): lax.all_to_all(outgoing, 'kv', split_axis=0, concat_axis=0, tiled=True)  6 us
    psum x1, blocking collectives, per_device(): squares = lax.psum(jnp.sum(attn_f32 * attn_f32, axis=1), 'tp')  5.63 us
    dot_general x4, matrix products, attend(): jnp.einsum('phqsk,pskd->pqhd', softmax_w, value_part, preferred_element_t...  4.94 us
    dynamic_slice x8, local copies, waits for them, and re-layouts, per_device(): lax.map(attend, (queries.reshape(pair_count, 2, BLK, head_count, HD), sel...  4.53 us
    dot_general x1, matrix products, per_device(): jnp.dot(jnp.concatenate(lax.all_gather(scaled, 'tp'), axis=1), w_out, pre...  2.75 us
  transfers between devices with their start and end apart: 3, of which 2 were waited for; matrix products, arithmetic and copies ran while one was open for 12% of the time, Pallas kernels for 0%

profile of v1, /device:TPU:0, one launch (start us, length us, event | category | flops | bytes accessed | tf_op | source)
XLA Modules:
  0.0 88.2 jit_solution(16616096739684033500)
XLA Ops:
  6.5 0.8 fusion.20
  7.4 0.7 compare_and_fusion.1
  8.2 0.7 copy.39
  8.9 7.3 %all-to-all-start = ((s32[8,1,1]{2,1,0:T(1,128)}), s32[8,1,1]{2,1,0:T(1,128)S(1)}, u32[]{:S(2)}, u32[]{:S(2)}) async-start(s32[8,1,1]{2,1,0:T(1,128)} %copy.39), calls=%async_computation | async-start | bytes 8192 | tf_op jit(solution)/shard_map/all_to_all | solution.py:63
  16.2 0.7 compare_select_fusion
  16.9 1.7 %convolution_bitcast_fusion.1 = f32[512,1,64]{0,2,1:T(8,128)S(1)} fusion(bf16[512,2048]{1,0:T(8,128)(2,1)S(1)} %copy-done, bf16[2048,64]{0,1:T(8,128)(2,1)} %param.11), kind=kOutput, calls=%fused_computation.26 | convolution fusion | flops 134217728 | bytes 2490368 | tf_op jit(solution)/shard_map/dot_general | solution.py:47
  19.6 0.8 convolution_convert_fusion
  20.4 2.0 %fusion.34 = f32[512,256]{0,1:T(8,128)S(1)} fusion(bf16[512,2048]{1,0:T(8,128)(2,1)S(1)} %copy-done, bf16[2048,256]{1,0:T(8,128)(2,1)} %param.10), kind=kOutput, calls=%fused_computation.93 | convolution fusion | flops 536870912 | bytes 3670016 | tf_op jit(solution)/shard_map/dot_general | solution.py:40
  22.9 1.6 %pad_maximum_fusion = bf16[4,2,64,4,64]{2,1,0,4,3:T(2,128)(2,1)} fusion(bf16[4,2,64,4,32]{2,1,0,4,3:T(2,128)(2,1)S(1)} %concatenate.35, bf16[4,2,64,4,32]{2,1,0,4,3:T(2,128)(2,1)S(1)} %concatenate.34), kind=kLoop, calls=%fused_computation.29 | loop fusion | flops 131072 | bytes 524288 | tf_op jit(solution)/shard_map/concatenate | solution.py:22
  25.9 0.7 broadcast_select_fusion
  26.6 6.0 %all-to-all-start.1 = ((bf16[8,64,128]{2,1,0:T(8,128)(2,1)}), bf16[8,64,128]{2,1,0:T(8,128)(2,1)S(1)}, u32[]{:S(2)}, u32[]{:S(2)}) async-start(bf16[8,64,128]{2,1,0:T(8,128)(2,1)} %broadcast_select_fusion), calls=%async_computation.1 | async-start | bytes 262144 | tf_op jit(solution)/shard_map/all_to_all | solution.py:71
  32.7 0.8 dynamic_slice.23
  33.4 6.5 %all-to-all-done.1 = bf16[8,64,128]{2,1,0:T(8,128)(2,1)S(1)} async-done(((bf16[8,64,128]{2,1,0:T(8,128)(2,1)}), bf16[8,64,128]{2,1,0:T(8,128)(2,1)S(1)}, u32[]{:S(2)}, u32[]{:S(2)}) %all-to-all-start.1) | async-done | bytes 131104 | tf_op jit(solution)/shard_map/all_to_all | solution.py:71
  40.1 0.7 gather_fusion.1
  40.8 17.1 %while.11 = (s32[]{:T(128)}, bf16[4,2,64,4,64]{2,4,3,1,0:T(8,128)(2,1)}, bf16[4,2,8,64,128]{4,3,2,1,0:T(8,128)(2,1)S(1)}, pred[4,2,8]{2,1,0:T(4,128)(4,1)S(1)}, ...) while((s32[]{:T(128)}, ...), condition=%wide.region_4.5_spmd.clone, body=%wide.region_1.4_spmd.clone.sunk | while | flops 69369872 | bytes 13193617 | solution.py:100
  41.8 1.0 %constant_dynamic-slice_fusion.4 = bf16[1,2,64,4,64]{2,1,0,4,3:T(2,128)(2,1)S(1)} fusion(bf16[4,2,64,4,64]{2,1,0,4,3:T(2,128)(2,1)} %get-tuple-element.185, s32[]{:T(128)} %get-tuple-element.171), kind=kLoop, calls=%fused_computation.18.clone.1 | loop fusion | bytes 131076 | tf_op jit(solution)/shard_map/while/body/jit(dynamic_index_in_dim)/dynamic_slice | solution.py:100
  43.9 1.2 %fusion.52 = bf16[4,2,64,4,64]{2,4,3,1,0:T(8,128)(2,1)} fusion(bf16[4,2,64,4,64]{2,4,3,1,0:T(8,128)(2,1)} %get-tuple-element.172, s32[]{:T(128)} %get-tuple-element.171, f32[2,4,64,8,64]{2,4,1,3,0:T(8,128)S(1)} %get-tuple-element.161, f32[2,4,64]{2,1,0:T(4,128)S(1)} %fusion.51, f32[2,4,64]{2,1,0:T(4,128)S(1)} %get-tuple-element.162, ...), kind=kOutput, calls=%fused_computation.10.clone.1 | convolution fusion | flops 34373632 | bytes 1446400 | tf_op jit(solution)/shard_map/while/body/eval_jaxpr/phqsk,pskd->pqhd/dot_general | solution.py:95
  46.1 1.0 %constant_dynamic-slice_fusion.4 = bf16[1,2,64,4,64]{2,1,0,4,3:T(2,128)(2,1)S(1)} fusion(bf16[4,2,64,4,64]{2,1,0,4,3:T(2,128)(2,1)} %get-tuple-element.185, s32[]{:T(128)} %get-tuple-element.171), kind=kLoop, calls=%fused_computation.18.clone.1 | loop fusion | bytes 131076 | tf_op jit(solution)/shard_map/while/body/jit(dynamic_index_in_dim)/dynamic_slice | solution.py:100
  48.1 1.2 %fusion.52 = bf16[4,2,64,4,64]{2,4,3,1,0:T(8,128)(2,1)} fusion(bf16[4,2,64,4,64]{2,4,3,1,0:T(8,128)(2,1)} %get-tuple-element.172, s32[]{:T(128)} %get-tuple-element.171, f32[2,4,64,8,64]{2,4,1,3,0:T(8,128)S(1)} %get-tuple-element.161, f32[2,4,64]{2,1,0:T(4,128)S(1)} %fusion.51, f32[2,4,64]{2,1,0:T(4,128)S(1)} %get-tuple-element.162, ...), kind=kOutput, calls=%fused_computation.10.clone.1 | convolution fusion | flops 34373632 | bytes 1446400 | tf_op jit(solution)/shard_map/while/body/eval_jaxpr/phqsk,pskd->pqhd/dot_general | solution.py:95
  49.7 0.6 copy-done.1
  50.4 1.0 %constant_dynamic-slice_fusion.4 = bf16[1,2,64,4,64]{2,1,0,4,3:T(2,128)(2,1)S(1)} fusion(bf16[4,2,64,4,64]{2,1,0,4,3:T(2,128)(2,1)} %get-tuple-element.185, s32[]{:T(128)} %get-tuple-element.171), kind=kLoop, calls=%fused_computation.18.clone.1 | loop fusion | bytes 131076 | tf_op jit(solution)/shard_map/while/body/jit(dynamic_index_in_dim)/dynamic_slice | solution.py:100
  52.4 1.2 %fusion.52 = bf16[4,2,64,4,64]{2,4,3,1,0:T(8,128)(2,1)} fusion(bf16[4,2,64,4,64]{2,4,3,1,0:T(8,128)(2,1)} %get-tuple-element.172, s32[]{:T(128)} %get-tuple-element.171, f32[2,4,64,8,64]{2,4,1,3,0:T(8,128)S(1)} %get-tuple-element.161, f32[2,4,64]{2,1,0:T(4,128)S(1)} %fusion.51, f32[2,4,64]{2,1,0:T(4,128)S(1)} %get-tuple-element.162, ...), kind=kOutput, calls=%fused_computation.10.clone.1 | convolution fusion | flops 34373632 | bytes 1446400 | tf_op jit(solution)/shard_map/while/body/eval_jaxpr/phqsk,pskd->pqhd/dot_general | solution.py:95
  54.7 1.0 %constant_dynamic-slice_fusion.4 = bf16[1,2,64,4,64]{2,1,0,4,3:T(2,128)(2,1)S(1)} fusion(bf16[4,2,64,4,64]{2,1,0,4,3:T(2,128)(2,1)} %get-tuple-element.185, s32[]{:T(128)} %get-tuple-element.171), kind=kLoop, calls=%fused_computation.18.clone.1 | loop fusion | bytes 131076 | tf_op jit(solution)/shard_map/while/body/jit(dynamic_index_in_dim)/dynamic_slice | solution.py:100
  56.7 1.2 %fusion.52 = bf16[4,2,64,4,64]{2,4,3,1,0:T(8,128)(2,1)} fusion(bf16[4,2,64,4,64]{2,4,3,1,0:T(8,128)(2,1)} %get-tuple-element.172, s32[]{:T(128)} %get-tuple-element.171, f32[2,4,64,8,64]{2,4,1,3,0:T(8,128)S(1)} %get-tuple-element.161, f32[2,4,64]{2,1,0:T(4,128)S(1)} %fusion.51, f32[2,4,64]{2,1,0:T(4,128)S(1)} %get-tuple-element.162, ...), kind=kOutput, calls=%fused_computation.10.clone.1 | convolution fusion | flops 34373632 | bytes 1446400 | tf_op jit(solution)/shard_map/while/body/eval_jaxpr/phqsk,pskd->pqhd/dot_general | solution.py:95
  57.9 1.3 %copy.44 = f32[4,2,64,4,64]{4,3,2,1,0:T(4,128)S(1)} copy(bf16[4,2,64,4,64]{2,4,3,1,0:T(8,128)(2,1)} %get-tuple-element.47) | data formatting | bytes 786432 | tf_op jit(solution)/shard_map/convert_element_type | solution.py:110
  59.3 1.4 %reshape.395 = f32[1,512,256]{2,1,0:T(8,128)} reshape(f32[4,2,64,4,64]{4,3,2,1,0:T(4,128)S(1)} %copy.44) | data formatting | bytes 1048576 | tf_op jit(solution)/shard_map/convert_element_type | solution.py:110
  60.7 1.8 %multiply_convert_fusion = bf16[1,512,256]{2,1,0:T(8,128)(2,1)} fusion(f32[1,512,256]{2,1,0:T(8,128)} %reshape.395, f32[256]{0:T(256)S(1)} %dynamic_slice.23), kind=kLoop, calls=%fused_computation.30 | loop fusion | flops 262144 | bytes 787456 | tf_op jit(solution)/shard_map/convert_element_type | solution.py:113
  62.5 1.2 %multiply_reduce_fusion = f32[4,2,64]{2,1,0:T(2,128)S(1)} fusion(bf16[4,2,64,4,64]{2,4,3,1,0:T(8,128)(2,1)} %get-tuple-element.47), kind=kLoop, calls=%fused_computation.28 | loop fusion | flops 392704 | bytes 264192 | tf_op jit(solution)/shard_map/reduce_sum | solution.py:111
  63.8 5.6 %psum.7 = f32[512]{0:T(512)S(1)} all-reduce(f32[512]{0:T(512)S(1)} %reduce_sum.21), channel_id=1, replica_groups=mesh['kv'=8,'tp'=4] {'tp'}, use_global_device_ids=true, to_apply=%region_6.7 | all-reduce | flops 512 | bytes 4096 | tf_op jit(solution)/shard_map/psum | solution.py:111
  69.4 7.7 %all-gather.2.cloned.1.call-done = bf16[4,512,256]{2,1,0:T(8,128)(2,1)} async-done(((bf16[1,512,256]{2,1,0:T(8,128)(2,1)}), bf16[4,512,256]{2,1,0:T(8,128)(2,1)}) %all-gather.2.cloned.1.call-update) | async-done | bytes 1048592 | tf_op jit(solution)/shard_map/all_gather | solution.py:115
  77.1 1.5 %copy.45 = bf16[4,512,256]{1,2,0:T(8,128)(2,1)S(1)} copy(bf16[4,512,256]{2,1,0:T(8,128)(2,1)} %all-gather.2.cloned.1.call-done) | data formatting | bytes 2097152 | tf_op jit(solution)/shard_map/all_gather | solution.py:115
  78.6 2.8 %fusion.10 = bf16[512,512]{1,0:T(8,128)(2,1)} fusion(bf16[512,1024]{0,1:T(8,128)(2,1)S(1)} %bitcast.158, bf16[1024,512]{1,0:T(8,128)(2,1)} %param.13, f32[512]{0:T(512)S(1)} %add_rsqrt_fusion), kind=kOutput, calls=%fused_computation.25 | convolution fusion | flops 537395200 | bytes 2623488 | tf_op jit(solution)/shard_map/dot_general | solution.py:114
  (84 shorter events, 10.5 us)
Async XLA Ops:
  6.5 10.4 %copy-start = (bf16[512,2048]{1,0:T(8,128)(2,1)S(1)}, bf16[512,2048]{1,0:T(8,128)(2,1)}, u32[]{:S(2)}) copy-start(bf16[512,2048]{1,0:T(8,128)(2,1)} %param.9) | copy-start | bytes 6291460
  6.5 13.0 %copy-start.3 = (bf16[2048,64]{0,1:T(8,128)(2,1)S(1)}, bf16[2048,64]{0,1:T(8,128)(2,1)}, u32[]{:S(2)}) copy-start(bf16[2048,64]{0,1:T(8,128)(2,1)} %param.12) | copy-start | bytes 786436
  8.9 15.9 %all-to-all-start = ((s32[8,1,1]{2,1,0:T(1,128)}), s32[8,1,1]{2,1,0:T(1,128)S(1)}, u32[]{:S(2)}, u32[]{:S(2)}) async-start(s32[8,1,1]{2,1,0:T(1,128)} %copy.39), calls=%async_computation | async-start | bytes 8192 | tf_op jit(solution)/shard_map/all_to_all | solution.py:63
  22.4 11.0 %copy-start.4 = (s32[1,8,8]{2,1,0:T(8,128)S(1)}, s32[1,8,8]{2,1,0:T(8,128)}, u32[]{:S(2)}) copy-start(s32[1,8,8]{2,1,0:T(8,128)} %param.15) | copy-start | bytes 772
  26.6 13.3 %all-to-all-start.1 = ((bf16[8,64,128]{2,1,0:T(8,128)(2,1)}), bf16[8,64,128]{2,1,0:T(8,128)(2,1)S(1)}, u32[]{:S(2)}, u32[]{:S(2)}) async-start(bf16[8,64,128]{2,1,0:T(8,128)(2,1)} %broadcast_select_fusion), calls=%async_computation.1 | async-start | bytes 262144 | tf_op jit(solution)/shard_map/all_to_all | solution.py:71
  32.6 44.6 %all-gather.2.cloned.1.call-start = ((), (), s32[]{:S(2)}) async-start(), calls=%async_computation.2 | async-start | bytes 1310720 | tf_op jit(solution)/shard_map/all_gather | solution.py:115
  40.8 1.0 %copy-start.1 = (bf16[4,2,8,64,128]{4,3,2,1,0:T(8,128)(2,1)}, bf16[4,2,8,64,128]{4,3,2,1,0:T(8,128)(2,1)S(1)}, u32[]{:S(2)}) copy-start(bf16[4,2,8,64,128]{4,3,2,1,0:T(8,128)(2,1)S(1)} %get-tuple-element.181) | copy-start | bytes 3145732 | tf_op jit(solution)/shard_map/while
  43.9 1.2 %copy-start.2 = (bf16[4,2,8,64,128]{4,3,2,1,0:T(8,128)(2,1)S(1)}, bf16[4,2,8,64,128]{4,3,2,1,0:T(8,128)(2,1)}, u32[]{:S(2)}) copy-start(bf16[4,2,8,64,128]{4,3,2,1,0:T(8,128)(2,1)} %copy-done.1) | copy-start | bytes 3145732 | tf_op jit(solution)/shard_map/while
  45.1 1.0 %copy-start.1 = (bf16[4,2,8,64,128]{4,3,2,1,0:T(8,128)(2,1)}, bf16[4,2,8,64,128]{4,3,2,1,0:T(8,128)(2,1)S(1)}, u32[]{:S(2)}) copy-start(bf16[4,2,8,64,128]{4,3,2,1,0:T(8,128)(2,1)S(1)} %get-tuple-element.181) | copy-start | bytes 3145732 | tf_op jit(solution)/shard_map/while
  48.1 1.2 %copy-start.2 = (bf16[4,2,8,64,128]{4,3,2,1,0:T(8,128)(2,1)S(1)}, bf16[4,2,8,64,128]{4,3,2,1,0:T(8,128)(2,1)}, u32[]{:S(2)}) copy-start(bf16[4,2,8,64,128]{4,3,2,1,0:T(8,128)(2,1)} %copy-done.1) | copy-start | bytes 3145732 | tf_op jit(solution)/shard_map/while
  49.4 1.0 %copy-start.1 = (bf16[4,2,8,64,128]{4,3,2,1,0:T(8,128)(2,1)}, bf16[4,2,8,64,128]{4,3,2,1,0:T(8,128)(2,1)S(1)}, u32[]{:S(2)}) copy-start(bf16[4,2,8,64,128]{4,3,2,1,0:T(8,128)(2,1)S(1)} %get-tuple-element.181) | copy-start | bytes 3145732 | tf_op jit(solution)/shard_map/while
  52.4 1.2 %copy-start.2 = (bf16[4,2,8,64,128]{4,3,2,1,0:T(8,128)(2,1)S(1)}, bf16[4,2,8,64,128]{4,3,2,1,0:T(8,128)(2,1)}, u32[]{:S(2)}) copy-start(bf16[4,2,8,64,128]{4,3,2,1,0:T(8,128)(2,1)} %copy-done.1) | copy-start | bytes 3145732 | tf_op jit(solution)/shard_map/while
  53.7 1.0 %copy-start.1 = (bf16[4,2,8,64,128]{4,3,2,1,0:T(8,128)(2,1)}, bf16[4,2,8,64,128]{4,3,2,1,0:T(8,128)(2,1)S(1)}, u32[]{:S(2)}) copy-start(bf16[4,2,8,64,128]{4,3,2,1,0:T(8,128)(2,1)S(1)} %get-tuple-element.181) | copy-start | bytes 3145732 | tf_op jit(solution)/shard_map/while
  56.7 1.2 %copy-start.2 = (bf16[4,2,8,64,128]{4,3,2,1,0:T(8,128)(2,1)S(1)}, bf16[4,2,8,64,128]{4,3,2,1,0:T(8,128)(2,1)}, u32[]{:S(2)}) copy-start(bf16[4,2,8,64,128]{4,3,2,1,0:T(8,128)(2,1)} %copy-done.1) | copy-start | bytes 3145732 | tf_op jit(solution)/shard_map/while
Sparse Core Ops, SparseCore 0:
  62.6 14.4 all-gather.1
